TPU v7x, 32 devices: a whole 2x2x4 slice. The times are simulated.
32 devices in a mesh: sp: 16 (over z, y, x), tp: 2 (over core).
Axes of the slice: x: 2, y: 2, z: 4, core: 2. Of those that a mesh axis runs over, the one named last changes fastest.
Arguments:
- queries: bfloat16 [4096, 1024], P('sp', 'tp'), may hold values from -100 to 100
- keys: bfloat16 [256, 4096], P('tp', 'sp'), may hold values from -5 to 5
- values: bfloat16 [256, 4096], P('tp', 'sp'), may hold values from -4.5 to 4.5
- gate_cache: float32 [8, 4096], P('tp', 'sp'), as said below
- documents: int32 [4096], P('sp'), may hold values from 0 to 2, never falling along the last dimension, each value on 1 to 2560 neighbouring positions
- residual: bfloat16 [4096, 2048], P(('sp', 'tp')), may hold values from -3 to 3
- out_weight: bfloat16 [1024, 2048], replicated, may hold values from -2 to 2
- mix_gain: bfloat16 [2048], replicated, may hold values from 0.099609375 to 1.8984375
- routes: int32 [4096, 4], P(('sp', 'tp')), may hold values from 0 to 31, all different within a row; in each aligned block of 128 rows (0 to 127, 128 to 255, ...) at most 32 rows name the same one
- route_weight: float32 [4096, 4], P(('sp', 'tp')), may hold values from 0.25 to 1
- expert_gate: bfloat16 [32, 2048, 512], P(('sp', 'tp')), may hold values from -0.125 to 0.125
- expert_up: bfloat16 [32, 2048, 512], P(('sp', 'tp')), may hold values from -0.125 to 0.125
- expert_down: bfloat16 [32, 512, 2048], P(('sp', 'tp')), may hold values from -0.25 to 0.25
- shared_gate: bfloat16 [2048, 512], replicated, may hold values from -0.125 to 0.125
- shared_up: bfloat16 [2048, 512], replicated, may hold values from -0.125 to 0.125
- shared_down: bfloat16 [512, 2048], replicated, may hold values from -0.25 to 0.25
- ffn_gain: bfloat16 [2048], replicated, may hold values from 0.099609375 to 1.8984375
Outputs:
- result: bfloat16 [4096, 2048], P(('sp', 'tp'))
Inputs may be any that keep to these rules, and one draw needn't show every extreme that they name: `gate_cache`: entry (h, j) is the sum of head h's log forget gates over positions 0 to j. `documents`: never falls along the positions; no document has more than 2560 positions. `routes`: each row names 4 different experts; in the rows of one device (aligned blocks of 128 rows) no expert is named more than 32 times, a bound that some block reaches.
All inputs are finite; a program needn't handle non-finite values.
Results may differ from a plain program's by a relative error of at most 0.013.
Values may be sent and summed in bfloat16 or wider, within the bound.
A program may use at most 256 MiB of HBM per device.

v0:
```python
import jax
import jax.numpy as jnp
from jax import lax
from jax.sharding import PartitionSpec as P

HD = 128
residual_scale = 2.0**0.25
norm_epsilon = 1e-05
masked_score = -1e30


def normalize(summed, gain_vector):
    row_mean = jnp.mean(summed, axis=-1, keepdims=True)
    centred = summed - row_mean
    spread = jnp.mean(centred * centred, axis=-1, keepdims=True)
    return (centred * lax.rsqrt(spread + norm_epsilon) * gain_vector.astype(jnp.float32)).astype(
        jnp.bfloat16
    )


def expert_block(arrived, expert_gate, expert_up, expert_down):
    own_count = expert_gate.shape[0]
    grouped = arrived.reshape(-1, own_count, arrived.shape[1], arrived.shape[2])
    gate_part = jnp.einsum(
        "nemd,edf->nemf", grouped, expert_gate, preferred_element_type=jnp.float32
    )
    up_part = jnp.einsum("nemd,edf->nemf", grouped, expert_up, preferred_element_type=jnp.float32)
    hidden = (jax.nn.silu(gate_part) * up_part).astype(jnp.bfloat16)
    produced = jnp.einsum("nemf,efd->nemd", hidden, expert_down, preferred_element_type=jnp.float32)
    return produced.astype(jnp.bfloat16).reshape(arrived.shape)


def local(
    queries,
    keys,
    values,
    gate_cache,
    documents,
    residual,
    out_weight,
    mix_gain,
    routes,
    route_weight,
    expert_gate,
    expert_up,
    expert_down,
    shared_gate,
    shared_up,
    shared_down,
    ffn_gain,
):
    tok_rows = queries.shape[0]
    local_heads = gate_cache.shape[0]
    kv_local = keys.shape[0] // HD
    group_size = local_heads // kv_local
    score_scale = HD ** (-0.5)
    seq_start = lax.axis_index("sp") * tok_rows
    query_pos = seq_start + jnp.arange(tok_rows, dtype=jnp.int32)
    query_last = seq_start + tok_rows - 1
    query_cum = jnp.transpose(gate_cache).reshape(tok_rows, kv_local, group_size)
    grouped_q = queries.reshape(tok_rows, kv_local, group_size, HD)
    all_cache, all_docs = (
        lax.all_gather(gate_cache, "sp", axis=1, tiled=True),
        lax.all_gather(documents.reshape(1, tok_rows), "sp", axis=1, tiled=True),
    )
    doc_line = all_docs[0]
    initial = (
        jnp.full((tok_rows, kv_local, group_size), masked_score, jnp.float32),
        jnp.zeros((tok_rows, kv_local, group_size), jnp.float32),
        jnp.zeros((tok_rows, kv_local, group_size, HD), jnp.float32),
    )
    key_piece = lax.all_gather(keys, "sp", axis=1, tiled=True)
    value_piece = lax.all_gather(values, "sp", axis=1, tiled=True)
    width_keys = key_piece.shape[1]
    key_cum = all_cache.reshape(kv_local, group_size, width_keys)

    def update(state):
        running_max, running_sum, numerator = state
        key_block = key_piece.reshape(kv_local, HD, width_keys)
        value_block = value_piece.reshape(kv_local, HD, width_keys)
        scores = (
            jnp.einsum("qagd,adk->qagk", grouped_q, key_block, preferred_element_type=jnp.float32)
            * score_scale
        )
        scores = scores + query_cum[..., None] - key_cum[None]
        key_pos = jnp.arange(width_keys, dtype=jnp.int32)
        allowed = (key_pos[None, :] <= query_pos[:, None]) & (
            doc_line[None, :] == documents[:, None]
        )
        allowed = allowed[:, None, None, :]
        scores = jnp.where(allowed, scores, masked_score)
        new_max = jnp.maximum(running_max, jnp.max(scores, axis=-1))
        weights = jnp.where(allowed, jnp.exp(scores - new_max[..., None]), 0.0)
        new_sum = jnp.sum(weights, axis=-1)
        added = jnp.einsum(
            "qagk,adk->qagd",
            weights.astype(jnp.bfloat16),
            value_block,
            preferred_element_type=jnp.float32,
        )
        return (new_max, new_sum, added)

    active = (jnp.int32(0) <= query_last) & (doc_line[width_keys - 1] >= documents[0])
    running_max, running_sum, numerator = lax.cond(active, update, lambda state: state, initial)
    attended = (
        (numerator / running_sum[..., None])
        .astype(jnp.bfloat16)
        .reshape(tok_rows, local_heads * HD)
    )
    token_heads = lax.all_to_all(attended, "tp", split_axis=0, concat_axis=1, tiled=True)
    mixed = jnp.dot(token_heads, out_weight, preferred_element_type=jnp.float32)
    mixed = lax.optimization_barrier(mixed.astype(jnp.bfloat16)).astype(jnp.float32)
    settled = normalize(residual_scale * residual.astype(jnp.float32) + mixed, mix_gain)
    row_count = settled.shape[0]
    width_model = settled.shape[1]
    top_count = routes.shape[1]
    expert_total = lax.axis_size(("sp", "tp")) * expert_gate.shape[0]
    capacity = row_count * lax.axis_size("tp") * top_count // expert_total
    chosen_experts = routes.reshape(-1)
    matches = (
        chosen_experts[:, None] == jnp.arange(expert_total, dtype=jnp.int32)[None, :]
    ).astype(jnp.int32)
    ranks = jnp.sum(jnp.cumsum(matches, axis=0) * matches, axis=1) - 1
    slots = chosen_experts * capacity + ranks
    placing = slots[None, :] == jnp.arange(expert_total * capacity, dtype=jnp.int32)[:, None]
    placing = jnp.any(
        placing.reshape(expert_total * capacity, row_count, top_count), axis=2
    ).astype(jnp.bfloat16)
    outgoing = jnp.dot(placing, settled, preferred_element_type=jnp.float32).astype(jnp.bfloat16)
    outgoing = outgoing.reshape(expert_total, capacity, width_model)
    finished = expert_block(
        lax.all_to_all(outgoing, ("sp", "tp"), split_axis=0, concat_axis=0, tiled=True),
        expert_gate,
        expert_up,
        expert_down,
    )
    returned = lax.all_to_all(finished, ("sp", "tp"), split_axis=0, concat_axis=0, tiled=True)
    returned = returned.reshape(expert_total * capacity, width_model)
    picked_rows = jnp.take(returned, slots, axis=0).reshape(row_count, top_count, width_model)
    routed = jnp.einsum("rkd,rk->rd", picked_rows.astype(jnp.float32), route_weight)
    shared_gate_part = jnp.dot(settled, shared_gate, preferred_element_type=jnp.float32)
    shared_up_part = jnp.dot(settled, shared_up, preferred_element_type=jnp.float32)
    shared_hidden = (jax.nn.silu(shared_gate_part) * shared_up_part).astype(jnp.bfloat16)
    shared = jnp.dot(shared_hidden, shared_down, preferred_element_type=jnp.float32)
    return normalize(residual_scale * settled.astype(jnp.float32) + routed + shared, ffn_gain)


def solution(mesh):
    placed = (
        P("sp", "tp"),
        P("tp", "sp"),
        P("tp", "sp"),
        P("tp", "sp"),
        P("sp"),
        P(("sp", "tp"), None),
        P(),
        P(),
        P(("sp", "tp"), None),
        P(("sp", "tp"), None),
        P(("sp", "tp"), None, None),
        P(("sp", "tp"), None, None),
        P(("sp", "tp"), None, None),
        P(),
        P(),
        P(),
        P(),
    )
    return jax.shard_map(
        local, mesh=mesh, in_specs=placed, out_specs=P(("sp", "tp"), None), check_vma=False
    )
```

profile of v0, /device:TPU:0, one launch (start us, length us, event | category | flops | bytes accessed | tf_op | source)
XLA Modules:
  0.0 393.6 jit_solution(2535516395564024456)
XLA Ops:
  6.5 1.7 copy.56
  8.3 0.7 all-gather.7.cloned.1.call-update
  9.0 0.8 copy.59
  9.8 0.1 eq.59
  9.9 0.1 reshape.234
  10.1 1.2 slice.14
  11.3 42.7 %all-gather.1 = s32[16,1,256]{2,1,0:T(1,128)S(1)} all-gather(s32[1,1,256]{2,1,0:T(1,128)} %bitcast.172), channel_id=2, replica_groups=mesh['sp'=16,'tp'=2] {'sp'}, dimensions={0}, use_global_device_ids=true | all-gather | bytes 17408 | tf_op jit(solution)/shard_map/all_gather | solution.py:64
  54.0 0.6 slice.19
  55.8 0.7 convert_element_type.60
  56.5 1.2 reduce-window.6
  57.7 0.2 slice_reduce_fusion
  58.0 0.1 fusion.50
  58.1 0.1 sub.47
  58.3 36.1 %all_gather.14 = f32[4,4096]{1,0:T(4,128)S(1)} all-gather(f32[4,256]{1,0:T(4,128)} %param.22), channel_id=1, replica_groups=mesh['sp'=16,'tp'=2] {'sp'}, dimensions={1}, use_global_device_ids=true | all-gather | bytes 69632 | tf_op jit(solution)/shard_map/all_gather | solution.py:63
  94.4 0.7 compare_and_fusion
  95.1 0.4 fusion.31
  95.4 29.3 %all-gather.7.cloned.1.call-done = bf16[128,4096]{1,0:T(8,128)(2,1)} async-done(((bf16[128,256]{1,0:T(8,128)(2,1)}), bf16[128,4096]{1,0:T(8,128)(2,1)}) %all-gather.7.cloned.1.call-update) | async-done | bytes 1048592 | tf_op jit(solution)/shard_map/all_gather | solution.py:73
  124.7 20.7 %conditional.1 = (f32[256,1,4]{0,2,1:T(4,128)S(1)}, f32[256,1,4,128]{3,0,2,1:T(8,128)S(1)}) conditional(s32[]{:T(128)} %convert_element_type.56, () %tuple.13, (s32[]{:T(128)}, s32[256]{0:T(256)S(1)}, s32[1,4096]{1,0:T(1,128)S(1)}, s32[256]{0:T(256)}, bf16[256,512]{1,0:T(8,128)(2,1)}, /*index=5*/bf16[128,4096]{0,1:T(8,128)(2,1)}, f32[256,4]{0,1:T(4,128)}, ...), branch_computations={%region_0.0_spmd, %region_1.4_spmd} | conditional | flops 2230320384 | bytes 61874252 | solution.py:104
  124.7 2.5 fusion.8
  127.3 5.5 %fusion.3 = (f32[256,4]{0,1:T(4,128)S(1)}, f32[4096,256,4]{1,0,2:T(8,128)S(1)}) fusion(f32[4,4096]{1,0:T(4,128)S(1)} %get-tuple-element.33, f32[256,4]{0,1:T(4,128)} %get-tuple-element.32, pred[256,4096]{0,1:T(8,128)(4,1)S(1)} %fusion.8, bf16[128,4096]{0,1:T(8,128)(2,1)} %get-tuple-element.30, bf16[256,512]{1,0:T(8,128)(2,1)} %get-tuple-element.40), kind=kOutput, calls=%fused_computation.7 | convolution fusion | flops 1094712320 | bytes 19210240 | tf_op jit(solution)/shard_map/cond/branch_1_fun/qagd,adk->qagk/dot_general | solution.py:82
  132.8 6.8 %fusion.9 = f32[256,1,4,128]{3,0,2,1:T(8,128)S(1)} fusion(f32[4096,256,4]{1,0,2:T(8,128)S(1)} %get-tuple-element.44, f32[256,4]{0,1:T(4,128)S(1)} %broadcast_maximum_fusion, f32[4,4096]{1,0:T(4,128)S(1)} %get-tuple-element.33, f32[256,4]{0,1:T(4,128)S(1)} %copy-done.5, pred[256,4096]{0,1:T(8,128)(4,1)S(1)} %fusion.8, bf16[128,4096]{1,0:T(8,128)(2,1)S(1)} %copy-done.9), kind=kOutput, calls=%fused_computation.13 | convolution fusion | flops 1103101952 | bytes 19472384 | tf_op jit(solution)/shard_map/cond/branch_1_fun/qagk,adk->qagd/dot_general | solution.py:95
  139.7 5.8 %fusion.2 = f32[256,4]{0,1:T(4,128)S(1)} fusion(f32[4096,256,4]{1,0,2:T(8,128)S(1)} %get-tuple-element.44, f32[256,4]{0,1:T(4,128)S(1)} %broadcast_maximum_fusion, f32[4,4096]{1,0:T(4,128)S(1)} %get-tuple-element.33, f32[256,4]{0,1:T(4,128)S(1)} %copy-done.5, pred[256,4096]{0,1:T(8,128)(4,1)S(1)} %fusion.8), kind=kLoop, calls=%fused_computation.6 | loop fusion | flops 29359104 | bytes 17903616 | tf_op jit(solution)/shard_map/cond/branch_1_fun/reduce_sum | solution.py:94
  145.5 0.2 divide_convert_fusion
  145.7 0.2 copy.57
  146.0 3.9 %all_to_all.29 = bf16[2,128,512]{2,1,0:T(8,128)(2,1)S(1)} all-to-all(bf16[2,128,512]{2,1,0:T(8,128)(2,1)S(1)} %all_to_all.20), channel_id=1, replica_groups=mesh['sp'=16,'tp'=2] {'tp'}, dimensions={0} | all-to-all | bytes 524288 | tf_op jit(solution)/shard_map/all_to_all | solution.py:110
  149.9 0.2 copy.58
  150.1 2.9 convolution_convert_fusion.2
  153.1 0.3 fusion.40
  153.3 0.3 multiply_reduce_fusion.1
  153.7 0.3 multiply_convert_fusion.1
  154.0 1.2 convolution_convert_fusion.1
  155.2 96.7 %all_to_all.30 = bf16[32,32,2048]{2,1,0:T(8,128)(2,1)S(1)} all-to-all(bf16[32,32,2048]{2,1,0:T(8,128)(2,1)S(1)} %bitcast.161), channel_id=1, replica_groups=mesh['sp'=16,'tp'=2] {'sp','tp'}, dimensions={0} | all-to-all | bytes 8388608 | tf_op jit(solution)/shard_map/all_to_all | solution.py:132
  252.0 2.0 copy-done.3
  253.9 3.7 fusion.22
  257.7 10.1 %convolution_convert_fusion = bf16[32,32,2048]{2,1,0:T(8,128)(2,1)} fusion(bf16[1,512,2048]{2,1,0:T(8,128)(2,1)S(1)} %copy-done, f32[32,32,512]{2,1,0:T(8,128)} %fusion.22, bf16[32,32,2048]{2,1,0:T(8,128)(2,1)} %copy-done.3, bf16[1,2048,512]{2,1,0:T(8,128)(2,1)} %param.29), kind=kOutput, calls=%fused_computation.24 | convolution fusion | flops 4300210176 | bytes 14680064 | tf_op jit(solution)/shard_map/nemf,efd->nemd/dot_general | solution.py:29
  267.7 4.0 %all-to-all-start.2 = ((bf16[32,32,2048]{2,1,0:T(8,128)(2,1)}), bf16[32,32,2048]{2,1,0:T(8,128)(2,1)}, u32[]{:S(2)}, u32[]{:S(2)}) async-start(bf16[32,32,2048]{2,1,0:T(8,128)(2,1)} %convolution_convert_fusion), calls=%async_computation.2 | async-start | bytes 8388608 | tf_op jit(solution)/shard_map/all_to_all | solution.py:137
  271.8 0.1 copy.64
  271.9 0.1 mul.107
  272.0 0.1 copy.63
  272.2 0.2 copy.66
  272.4 2.0 fusion.58
  274.4 91.0 %all-to-all-done.2 = bf16[32,32,2048]{2,1,0:T(8,128)(2,1)} async-done(((bf16[32,32,2048]{2,1,0:T(8,128)(2,1)}), bf16[32,32,2048]{2,1,0:T(8,128)(2,1)}, u32[]{:S(2)}, u32[]{:S(2)}) %all-to-all-start.2) | async-done | bytes 4194336 | tf_op jit(solution)/shard_map/all_to_all | solution.py:137
  365.5 8.0 %gather_fusion = bf16[512,2048]{1,0:T(8,128)(2,1)} fusion(bf16[1024,2048]{1,0:T(8,128)(2,1)} %bitcast.35, s32[1024]{0:T(1024)S(1)} %pad_clamp_fusion), kind=kCustom, calls=%fused_computation | custom fusion | bytes 4196352 | tf_op jit(solution)/shard_map/jit(_take)/gather | solution.py:139
  373.5 4.1 %gather.7 = bf16[128,4,2048]{2,1,0:T(4,128)(2,1)} reshape(bf16[512,2048]{1,0:T(8,128)(2,1)} %gather_fusion) | data formatting | bytes 4194304 | tf_op jit(solution)/shard_map/jit(_take)/gather | solution.py:139
  377.6 3.9 fusion.29
  381.5 4.0 %fusion.57 = (f32[128]{0:T(128)S(1)}, f32[128,2048]{1,0:T(8,128)S(1)}) fusion(bf16[512,2048]{1,0:T(8,128)(2,1)} %param.34, bf16[128,2048]{1,0:T(8,128)(2,1)} %copy-done.1, bf16[2048,512]{1,0:T(8,128)(2,1)} %param.33, f32[128,512]{1,0:T(8,128)S(1)} %fusion.58, f32[128,1,2048]{2,1,0:T(1,128)} %fusion.29), kind=kOutput, calls=%fused_computation.85 | convolution fusion | flops 538574720 | bytes 7078400 | tf_op jit(solution)/shard_map/dot_general | solution.py:144
  385.5 0.3 multiply_reduce_fusion
  385.7 1.0 multiply_convert_fusion
  (40 shorter events, 0.4 us)
Async XLA Ops:
  6.5 251.1 %copy-start = (bf16[1,512,2048]{2,1,0:T(8,128)(2,1)S(1)}, bf16[1,512,2048]{2,1,0:T(8,128)(2,1)}, u32[]{:S(2)}) copy-start(bf16[1,512,2048]{2,1,0:T(8,128)(2,1)} %param.31) | copy-start | bytes 6291460
  6.5 88.9 %all-gather.5.cloned.1.call-start = ((), (), s32[]{:S(2)}) async-start(), calls=%async_computation.3 | async-start | bytes 1114112 | tf_op jit(solution)/shard_map/all_gather | solution.py:72
  8.3 116.4 %all-gather.7.cloned.1.call-start = ((), (), s32[]{:S(2)}) async-start(), calls=%async_computation.4 | async-start | bytes 1114112 | tf_op jit(solution)/shard_map/all_gather | solution.py:73
  127.3 5.5 %copy-start.5 = (f32[256,4]{0,1:T(4,128)S(1)}, f32[256,4]{0,1:T(4,128)}, u32[]{:S(2)}) copy-start(f32[256,4]{0,1:T(4,128)} %get-tuple-element.32) | copy-start | bytes 12292 | tf_op jit(solution)/shard_map/cond
  127.3 5.5 %copy-start.9 = (bf16[128,4096]{1,0:T(8,128)(2,1)S(1)}, bf16[128,4096]{1,0:T(8,128)(2,1)}, u32[]{:S(2)}) copy-start(bf16[128,4096]{1,0:T(8,128)(2,1)} %get-tuple-element.34) | copy-start | bytes 3145732 | tf_op jit(solution)/shard_map/cond
  145.5 7.6 %copy-start.2 = (bf16[128,2048]{1,0:T(8,128)(2,1)S(1)}, bf16[128,2048]{1,0:T(8,128)(2,1)}, u32[]{:S(2)}) copy-start(bf16[128,2048]{1,0:T(8,128)(2,1)} %param.24) | copy-start | bytes 1572868
  154.0 118.4 %copy-start.1 = (bf16[128,2048]{1,0:T(8,128)(2,1)}, bf16[128,2048]{1,0:T(8,128)(2,1)S(1)}, u32[]{:S(2)}) copy-start(bf16[128,2048]{1,0:T(8,128)(2,1)S(1)} %multiply_convert_fusion.1) | copy-start | bytes 1572868
  155.2 98.7 %copy-start.8 = (bf16[1,2048,512]{2,1,0:T(8,128)(2,1)S(1)}, bf16[1,2048,512]{2,1,0:T(8,128)(2,1)}, u32[]{:S(2)}) copy-start(bf16[1,2048,512]{2,1,0:T(8,128)(2,1)} %param.30) | copy-start | bytes 6291460
  252.0 2.0 copy-start.3
  267.7 4.0 %copy-start.4 = (s32[128,4]{0,1:T(4,128)S(1)}, s32[128,4]{0,1:T(4,128)}, u32[]{:S(2)}) copy-start(s32[128,4]{0,1:T(4,128)} %param.27) | copy-start | bytes 6148
  267.7 4.4 %copy-start.7 = (f32[128,4]{0,1:T(4,128)S(1)}, f32[128,4]{0,1:T(4,128)}, u32[]{:S(2)}) copy-start(f32[128,4]{0,1:T(4,128)} %param.28) | copy-start | bytes 6148
  267.7 4.6 %copy-start.6 = (bf16[2048]{0:T(1024)(128)(2,1)S(1)}, bf16[2048]{0:T(1024)(128)(2,1)}, u32[]{:S(2)}) copy-start(bf16[2048]{0:T(1024)(128)(2,1)} %param.35) | copy-start | bytes 12292
  267.7 97.7 %all-to-all-start.2 = ((bf16[32,32,2048]{2,1,0:T(8,128)(2,1)}), bf16[32,32,2048]{2,1,0:T(8,128)(2,1)}, u32[]{:S(2)}, u32[]{:S(2)}) async-start(bf16[32,32,2048]{2,1,0:T(8,128)(2,1)} %convolution_convert_fusion), calls=%async_computation.2 | async-start | bytes 8388608 | tf_op jit(solution)/shard_map/all_to_all | solution.py:137
Sparse Core Ops, SparseCore 0:
  10.1 57.9 all-gather.4
  70.8 53.9 all-gather.6
where the time goes:
time: 394 us
  blocking collectives  180 us (46%)
  waiting for transfers between devices  121 us (31%)
  matrix products  40.2 us (10%)
  local copies, waits for them, and re-layouts  20.1 us (5%)
  between operations  14.9 us (4%)
  other arithmetic  13.8 us (4%)
  starting transfers between devices  4.06 us (1%)
    all_to_all x1, blocking collectives, local(): lax.all_to_all(outgoing, ('sp', 'tp'), split_axis=0, concat_axis=0, tiled...  96.7 us
    all_to_all x1, waiting for transfers between devices, local(): lax.all_to_all(finished, ('sp', 'tp'), split_axis=0, concat_axis=0, tiled...  91 us
    all_gather x1, blocking collectives, local(): lax.all_gather(documents.reshape(1, tok_rows), 'sp', axis=1, tiled=True)  42.7 us
    all_gather x1, blocking collectives, local(): lax.all_gather(gate_cache, 'sp', axis=1, tiled=True)  36.1 us
    all_gather x1, waiting for transfers between devices, local(): value_piece = lax.all_gather(values, 'sp', axis=1, tiled=True)  29.3 us
    gather x2, local copies, waits for them, and re-layouts, local(): jnp.take(returned, slots, axis=0).reshape(row_count, top_count, width_model)  12.1 us
    dot_general x1, matrix products, expert_block(): jnp.einsum('nemf,efd->nemd', hidden, expert_down, preferred_element_type=...  10.1 us
  transfers between devices with their start and end apart: 3, of which 2 were waited for; matrix products, arithmetic and copies ran while one was open for 2% of the time, Pallas kernels for 0%

commit v1 on v0

--- a/solution.py
+++ b/solution.py
@@ -69,8 +69,11 @@
         jnp.zeros((tok_rows, kv_local, group_size), jnp.float32),
         jnp.zeros((tok_rows, kv_local, group_size, HD), jnp.float32),
     )
-    key_piece = lax.all_gather(keys, "sp", axis=1, tiled=True)
-    value_piece = lax.all_gather(values, "sp", axis=1, tiled=True)
+    key_piece, value_piece = jnp.split(
+        lax.all_gather(jnp.concatenate([keys, values], axis=0), "sp", axis=1, tiled=True),
+        [keys.shape[0]],
+        axis=0,
+    )
     width_keys = key_piece.shape[1]
     key_cum = all_cache.reshape(kv_local, group_size, width_keys)
 

time: 394 us -> 379 us (0.962)
  waiting for transfers between devices: 121 us -> 91.1 us
  matrix products: 40.2 us -> 49.2 us
  local copies, waits for them, and re-layouts: 20.1 us -> 24.5 us
    all_gather x2 -> x1, waiting for transfers between devices: 29.3 us -> 0.02 us  [local(): lax.all_gather(jnp.concatenate([keys, values], axis=0), 'sp', axis=1, til...]
    dot_general x1, matrix products: 6.82 us -> 11.6 us  [update(): jnp.einsum('qagk,adk->qagd', weights.astype(jnp.bfloat16), value_block, p...]
    dot_general x1, matrix products: 5.47 us -> 9.79 us  [update(): jnp.einsum('qagd,adk->qagk', grouped_q, key_block, preferred_element_type...]
    another operation x1 -> x2, local copies, waits for them, and re-layouts: 0.01 us -> 4.13 us
  transfers between devices with their start and end apart: 3 -> 2, of which waited for: 2 -> 1; matrix products, arithmetic and copies ran while one was open for 2% -> 2% of each run, Pallas kernels for 0% -> 0%
where the time goes in v1:
time: 379 us; the launch traced here: 378 us
  blocking collectives  179 us (47%)
  waiting for transfers between devices  91.1 us (24%)
  matrix products  49.2 us (13%)
  local copies, waits for them, and re-layouts  24.5 us (6%)
  other arithmetic  15.7 us (4%)
  between operations  14.9 us (4%)
  starting transfers between devices  3.8 us (1%)
    all_to_all x1, blocking collectives, local(): lax.all_to_all(outgoing, ('sp', 'tp'), split_axis=0, concat_axis=0, tiled...  95.6 us
    all_to_all x1, waiting for transfers between devices, local(): lax.all_to_all(finished, ('sp', 'tp'), split_axis=0, concat_axis=0, tiled...  91 us
    all_gather x1, blocking collectives, local(): lax.all_gather(documents.reshape(1, tok_rows), 'sp', axis=1, tiled=True)  42.8 us
    all_gather x1, blocking collectives, local(): lax.all_gather(gate_cache, 'sp', axis=1, tiled=True)  36.5 us
    gather x2, local copies, waits for them, and re-layouts, local(): jnp.take(returned, slots, axis=0).reshape(row_count, top_count, width_model)  12.1 us
    dot_general x1, matrix products, update(): jnp.einsum('qagk,adk->qagd', weights.astype(jnp.bfloat16), value_block, p...  11.6 us
    dot_general x1, matrix products, expert_block(): jnp.einsum('nemf,efd->nemd', hidden, expert_down, preferred_element_type=...  10 us
    dot_general x1, matrix products, update(): jnp.einsum('qagd,adk->qagk', grouped_q, key_block, preferred_element_type...  9.79 us
  transfers between devices with their start and end apart: 2, of which 1 were waited for; matrix products, arithmetic and copies ran while one was open for 2% of the time, Pallas kernels for 0%

profile of v1, /device:TPU:0, one launch (start us, length us, event | category | flops | bytes accessed | tf_op | source)
XLA Modules:
  0.0 378.1 jit_solution(15300692476622716140)
XLA Ops:
  6.5 1.1 copy.65
  7.6 1.0 copy.66
  8.6 0.7 pad_maximum_fusion
  9.3 0.8 copy.69
  10.2 0.1 reshape.234
  10.3 1.2 slice.14
  11.5 42.8 %all-gather.1 = s32[16,1,256]{2,1,0:T(1,128)S(1)} all-gather(s32[1,1,256]{2,1,0:T(1,128)} %bitcast.172), channel_id=2, replica_groups=mesh['sp'=16,'tp'=2] {'sp'}, dimensions={0}, use_global_device_ids=true | all-gather | bytes 17408 | tf_op jit(solution)/shard_map/all_gather | solution.py:64
  54.3 0.6 slice.19
  56.2 0.7 convert_element_type.60
  56.9 1.2 reduce-window.6
  58.0 0.2 slice_reduce_fusion
  58.3 0.1 fusion.50
  58.4 0.1 sub.47
  58.6 36.5 %all_gather.11 = f32[4,4096]{1,0:T(4,128)S(1)} all-gather(f32[4,256]{1,0:T(4,128)} %param.22), channel_id=1, replica_groups=mesh['sp'=16,'tp'=2] {'sp'}, dimensions={1}, use_global_device_ids=true | all-gather | bytes 69632 | tf_op jit(solution)/shard_map/all_gather | solution.py:63
  95.1 0.7 compare_and_fusion
  95.8 0.4 fusion.31
  96.2 33.9 %conditional.1 = (f32[256,1,4]{0,2,1:T(4,128)S(1)}, f32[256,1,4,128]{3,0,2,1:T(8,128)}) conditional(s32[]{:T(128)} %convert_element_type.56, () %tuple.13, (s32[]{:T(128)}, s32[256]{0:T(256)S(1)}, s32[1,4096]{1,0:T(1,128)S(1)}, s32[256]{0:T(256)}, bf16[256,4096]{0,1:T(8,128)(2,1)}, /*index=5*/bf16[256,512]{1,0:T(8,128)(2,1)}, f32[256,4]{0,1:T(4,128)}, ...), branch_computations={%region_0.0_spmd, %region_1.4_spmd} | conditional | flops 2230320384 | bytes 128983112 | solution.py:107
  96.2 2.6 fusion.8
  98.8 9.8 %fusion.3 = (f32[256,4]{0,1:T(4,128)S(1)}, f32[4096,256,4]{1,0,2:T(8,128)}) fusion(f32[4,4096]{1,0:T(4,128)S(1)} %get-tuple-element.34, f32[256,4]{0,1:T(4,128)} %get-tuple-element.33, pred[256,4096]{0,1:T(8,128)(4,1)S(1)} %fusion.8, bf16[256,4096]{0,1:T(8,128)(2,1)} %get-tuple-element.31, bf16[256,512]{1,0:T(8,128)(2,1)} %get-tuple-element.40), kind=kOutput, calls=%fused_computation.7 | convolution fusion | flops 1094712320 | bytes 19210240 | tf_op jit(solution)/shard_map/cond/branch_1_fun/qagd,adk->qagk/dot_general | solution.py:85
  108.6 4.1 %copy.63 = bf16[256,4096]{1,0:T(8,128)(2,1)} copy(bf16[256,4096]{0,1:T(8,128)(2,1)} %get-tuple-element.31) | data formatting | bytes 4194304 | tf_op jit(solution)/shard_map
  112.7 11.6 %fusion.9 = f32[256,1,4,128]{3,0,2,1:T(8,128)} fusion(f32[4096,256,4]{1,0,2:T(8,128)} %get-tuple-element.44, f32[256,4]{0,1:T(4,128)S(1)} %broadcast_maximum_fusion, f32[4,4096]{1,0:T(4,128)S(1)} %get-tuple-element.34, f32[256,4]{0,1:T(4,128)S(1)} %copy-done.6, pred[256,4096]{0,1:T(8,128)(4,1)S(1)} %fusion.8, bf16[256,4096]{1,0:T(8,128)(2,1)} %copy.63), kind=kOutput, calls=%fused_computation.13 | convolution fusion | flops 1103101952 | bytes 19472384 | tf_op jit(solution)/shard_map/cond/branch_1_fun/qagk,adk->qagd/dot_general | solution.py:98
  124.3 5.8 %fusion.2 = f32[256,4]{0,1:T(4,128)S(1)} fusion(f32[4096,256,4]{1,0,2:T(8,128)S(1)} %copy-done.1, f32[256,4]{0,1:T(4,128)S(1)} %broadcast_maximum_fusion, f32[4,4096]{1,0:T(4,128)S(1)} %get-tuple-element.34, f32[256,4]{0,1:T(4,128)S(1)} %copy-done.6, pred[256,4096]{0,1:T(8,128)(4,1)S(1)} %fusion.8), kind=kLoop, calls=%fused_computation.6 | loop fusion | flops 29359104 | bytes 17903616 | tf_op jit(solution)/shard_map/cond/branch_1_fun/reduce_sum | solution.py:97
  130.1 1.3 divide_convert_fusion
  131.5 0.2 copy.67
  131.8 3.9 %all_to_all.29 = bf16[2,128,512]{2,1,0:T(8,128)(2,1)S(1)} all-to-all(bf16[2,128,512]{2,1,0:T(8,128)(2,1)S(1)} %all_to_all.20), channel_id=1, replica_groups=mesh['sp'=16,'tp'=2] {'tp'}, dimensions={0} | all-to-all | bytes 524288 | tf_op jit(solution)/shard_map/all_to_all | solution.py:113
  135.7 0.2 copy.68
  135.9 2.9 convolution_convert_fusion.2
  138.8 0.3 fusion.40
  139.1 0.3 multiply_reduce_fusion.1
  139.4 0.3 multiply_convert_fusion.1
  139.8 1.2 convolution_convert_fusion.1
  141.0 95.6 %all_to_all.30 = bf16[32,32,2048]{2,1,0:T(8,128)(2,1)S(1)} all-to-all(bf16[32,32,2048]{2,1,0:T(8,128)(2,1)S(1)} %bitcast.161), channel_id=1, replica_groups=mesh['sp'=16,'tp'=2] {'sp','tp'}, dimensions={0} | all-to-all | bytes 8388608 | tf_op jit(solution)/shard_map/all_to_all | solution.py:135
  236.6 2.0 copy-done.4
  238.6 3.7 fusion.22
  242.3 10.0 %convolution_convert_fusion = bf16[32,32,2048]{2,1,0:T(8,128)(2,1)} fusion(bf16[1,512,2048]{2,1,0:T(8,128)(2,1)S(1)} %copy-done, f32[32,32,512]{2,1,0:T(8,128)} %fusion.22, bf16[32,32,2048]{2,1,0:T(8,128)(2,1)} %copy-done.4, bf16[1,2048,512]{2,1,0:T(8,128)(2,1)} %param.29), kind=kOutput, calls=%fused_computation.25 | convolution fusion | flops 4300210176 | bytes 14680064 | tf_op jit(solution)/shard_map/nemf,efd->nemd/dot_general | solution.py:29
  252.4 3.8 %all-to-all-start.2 = ((bf16[32,32,2048]{2,1,0:T(8,128)(2,1)}), bf16[32,32,2048]{2,1,0:T(8,128)(2,1)}, u32[]{:S(2)}, u32[]{:S(2)}) async-start(bf16[32,32,2048]{2,1,0:T(8,128)(2,1)} %convolution_convert_fusion), calls=%async_computation.2 | async-start | bytes 8388608 | tf_op jit(solution)/shard_map/all_to_all | solution.py:140
  256.2 0.1 copy.74
  256.3 0.1 mul.107
  256.4 0.1 copy.73
  256.6 0.2 copy.76
  256.8 2.0 fusion.58
  258.8 91.0 %all-to-all-done.2 = bf16[32,32,2048]{2,1,0:T(8,128)(2,1)} async-done(((bf16[32,32,2048]{2,1,0:T(8,128)(2,1)}), bf16[32,32,2048]{2,1,0:T(8,128)(2,1)}, u32[]{:S(2)}, u32[]{:S(2)}) %all-to-all-start.2) | async-done | bytes 4194336 | tf_op jit(solution)/shard_map/all_to_all | solution.py:140
  349.9 8.0 %gather_fusion = bf16[512,2048]{1,0:T(8,128)(2,1)} fusion(bf16[1024,2048]{1,0:T(8,128)(2,1)} %bitcast.35, s32[1024]{0:T(1024)S(1)} %pad_clamp_fusion), kind=kCustom, calls=%fused_computation | custom fusion | bytes 4196352 | tf_op jit(solution)/shard_map/jit(_take)/gather | solution.py:142
  357.9 4.1 %gather.7 = bf16[128,4,2048]{2,1,0:T(4,128)(2,1)} reshape(bf16[512,2048]{1,0:T(8,128)(2,1)} %gather_fusion) | data formatting | bytes 4194304 | tf_op jit(solution)/shard_map/jit(_take)/gather | solution.py:142
  362.0 3.9 %fusion.29 = f32[128,1,2048]{2,1,0:T(1,128)} fusion(bf16[128,4,1]{1,2,0:T(2,128)(2,1)S(1)} %copy.76, bf16[128,4,2048]{2,1,0:T(4,128)(2,1)} %gather.7, pred[128,4]{1,0:T(8,128)(4,1)S(1)} %copy.73), kind=kOutput, calls=%fused_computation.42 | convolution fusion | flops 3145728 | bytes 3147264 | tf_op jit(solution)/shard_map/rkd,rk->rd/dot_general | solution.py:143
  365.9 4.0 %fusion.57 = (f32[128]{0:T(128)S(1)}, f32[128,2048]{1,0:T(8,128)S(1)}) fusion(bf16[512,2048]{1,0:T(8,128)(2,1)} %param.34, bf16[128,2048]{1,0:T(8,128)(2,1)} %copy-done.2, bf16[2048,512]{1,0:T(8,128)(2,1)} %param.33, f32[128,512]{1,0:T(8,128)S(1)} %fusion.58, f32[128,1,2048]{2,1,0:T(1,128)} %fusion.29), kind=kOutput, calls=%fused_computation.87 | convolution fusion | flops 538574720 | bytes 7078400 | tf_op jit(solution)/shard_map/dot_general | solution.py:147
  369.9 0.3 multiply_reduce_fusion
  370.2 1.0 multiply_convert_fusion
  (40 shorter events, 0.5 us)
Async XLA Ops:
  6.5 235.8 %copy-start = (bf16[1,512,2048]{2,1,0:T(8,128)(2,1)S(1)}, bf16[1,512,2048]{2,1,0:T(8,128)(2,1)}, u32[]{:S(2)}) copy-start(bf16[1,512,2048]{2,1,0:T(8,128)(2,1)} %param.31) | copy-start | bytes 6291460
  6.5 89.6 %all-gather.4.cloned.1.call-start = ((), (), s32[]{:S(2)}) async-start(), calls=%async_computation.3 | async-start | bytes 2228224 | tf_op jit(solution)/shard_map/all_gather | solution.py:73
  108.6 4.1 %copy-start.6 = (f32[256,4]{0,1:T(4,128)S(1)}, f32[256,4]{0,1:T(4,128)}, u32[]{:S(2)}) copy-start(f32[256,4]{0,1:T(4,128)} %get-tuple-element.33) | copy-start | bytes 12292 | tf_op jit(solution)/shard_map/cond
  112.7 11.6 %copy-start.1 = (f32[4096,256,4]{1,0,2:T(8,128)S(1)}, f32[4096,256,4]{1,0,2:T(8,128)}, u32[]{:S(2)}) copy-start(f32[4096,256,4]{1,0,2:T(8,128)} %get-tuple-element.44) | copy-start | bytes 50331652 | tf_op jit(solution)/shard_map/cond
  130.1 8.7 %copy-start.3 = (bf16[128,2048]{1,0:T(8,128)(2,1)S(1)}, bf16[128,2048]{1,0:T(8,128)(2,1)}, u32[]{:S(2)}) copy-start(bf16[128,2048]{1,0:T(8,128)(2,1)} %param.24) | copy-start | bytes 1572868
  139.7 117.0 %copy-start.2 = (bf16[128,2048]{1,0:T(8,128)(2,1)}, bf16[128,2048]{1,0:T(8,128)(2,1)S(1)}, u32[]{:S(2)}) copy-start(bf16[128,2048]{1,0:T(8,128)(2,1)S(1)} %multiply_convert_fusion.1) | copy-start | bytes 1572868
  141.0 97.6 %copy-start.9 = (bf16[1,2048,512]{2,1,0:T(8,128)(2,1)S(1)}, bf16[1,2048,512]{2,1,0:T(8,128)(2,1)}, u32[]{:S(2)}) copy-start(bf16[1,2048,512]{2,1,0:T(8,128)(2,1)} %param.30) | copy-start | bytes 6291460
  236.6 2.0 copy-start.4
  252.4 3.8 %copy-start.5 = (s32[128,4]{0,1:T(4,128)S(1)}, s32[128,4]{0,1:T(4,128)}, u32[]{:S(2)}) copy-start(s32[128,4]{0,1:T(4,128)} %param.27) | copy-start | bytes 6148
  252.4 4.2 %copy-start.8 = (f32[128,4]{0,1:T(4,128)S(1)}, f32[128,4]{0,1:T(4,128)}, u32[]{:S(2)}) copy-start(f32[128,4]{0,1:T(4,128)} %param.28) | copy-start | bytes 6148
  252.4 4.4 %copy-start.7 = (bf16[2048]{0:T(1024)(128)(2,1)S(1)}, bf16[2048]{0:T(1024)(128)(2,1)}, u32[]{:S(2)}) copy-start(bf16[2048]{0:T(1024)(128)(2,1)} %param.35) | copy-start | bytes 12292
  252.4 97.5 %all-to-all-start.2 = ((bf16[32,32,2048]{2,1,0:T(8,128)(2,1)}), bf16[32,32,2048]{2,1,0:T(8,128)(2,1)}, u32[]{:S(2)}, u32[]{:S(2)}) async-start(bf16[32,32,2048]{2,1,0:T(8,128)(2,1)} %convolution_convert_fusion), calls=%async_computation.2 | async-start | bytes 8388608 | tf_op jit(solution)/shard_map/all_to_all | solution.py:140
Sparse Core Ops, SparseCore 0:
  10.1 63.3 all-gather.3
